TPU v7x, 256 devices: a whole 4x4x8 slice. The times are simulated.
256 devices in a mesh: sp: 16 (over y, x), tp: 16 (over z, core).
Axes of the slice: x: 4, y: 4, z: 8, core: 2. Of those that a mesh axis runs over, the one named last changes fastest.
Arguments:
- gate_b: bfloat16 [8192, 1024], P('sp', 'tp'), may hold values from -6 to 6
- gate_c: bfloat16 [8192, 1024], P('sp', 'tp'), may hold values from -6 to 6
- values_in: bfloat16 [8192, 1024], P('sp', 'tp'), may hold values from -6 to 6
- conv_w: bfloat16 [3, 1024], P(None, 'tp'), may hold values from -3.5 to 3.5
- documents: int32 [8192], P('sp'), may hold values from 0 to 8, never falling along the last dimension, each value on 1 to 4096 neighbouring positions
- w_out: bfloat16 [1024, 2048], replicated, may hold values from -0.1875 to 0.1875
- resid: bfloat16 [8192, 2048], P(('sp', 'tp')), may hold values from -6 to 6
- norm_gain: bfloat16 [2048], replicated, may hold values from 0.099609375 to 1.8984375
- route_ids: int32 [8192, 2], P(('sp', 'tp')), may hold values from 0 to 15, all different within a row; in each aligned block of 32 rows (0 to 31, 32 to 63, ...) at most 8 rows name the same one
- route_weight: float32 [8192, 2], P(('sp', 'tp')), may hold values from 0.2 to 1
- w_gate: bfloat16 [16, 2048, 7168], P('sp', None, 'tp'), may hold values from -0.125 to 0.125
- w_up: bfloat16 [16, 2048, 7168], P('sp', None, 'tp'), may hold values from -0.125 to 0.125
- w_down: bfloat16 [16, 7168, 2048], P('sp', 'tp'), may hold values from -0.0625 to 0.0625
Outputs:
- layer_out: bfloat16 [8192, 2048], P(('sp', 'tp'))
Inputs may be any that keep to these rules, and one draw needn't show every extreme that they name: `route_ids`: each token names two different experts; in the rows of one device no expert is named by more than 8 rows, a bound that some block reaches. `documents`: document numbers never fall along the positions; a document has at most 8192 // 2 positions.
All inputs are finite; a program needn't handle non-finite values.
Results may differ from a plain program's by a relative error of at most 0.018.
Values may be sent and summed in bfloat16 or wider, within the bound.
A program may use at most 128 MiB of HBM per device.

v0:
```python
import jax
import jax.numpy as jnp
from jax import lax
from jax.sharding import PartitionSpec as P


def passed_along(block, axis, distance):
    devices = range(lax.axis_size(axis))
    route = [(i - distance, i) for i in devices if i - distance in devices]
    return lax.ppermute(block, axis, route)


def local(
    gate_b,
    gate_c,
    values_in,
    conv_w,
    documents,
    w_out,
    resid,
    norm_gain,
    route_ids,
    route_weight,
    w_gate,
    w_up,
    w_down,
):
    seq_rows = gate_b.shape[0]
    local_rows = resid.shape[0]
    model_width = resid.shape[1]
    last_rows = jnp.stack([gate_c[seq_rows - 2 :], values_in[seq_rows - 2 :]])
    before, before_docs = passed_along((last_rows, documents[seq_rows - 2 :]), "sp", 1)
    products = jnp.concatenate(
        [
            before[0].astype(jnp.float32) * before[1].astype(jnp.float32),
            gate_c.astype(jnp.float32) * values_in.astype(jnp.float32),
        ],
        axis=0,
    )
    docs_all = jnp.concatenate([before_docs, documents], axis=0)
    kernel_taps = conv_w.astype(jnp.float32)
    near_mask = (docs_all[1:-1] == documents).astype(jnp.float32)[:, None]
    far_mask = (docs_all[:-2] == documents).astype(jnp.float32)[:, None]
    convolved = (
        kernel_taps[2] * products[2:]
        + kernel_taps[1] * products[1:-1] * near_mask
        + kernel_taps[0] * products[:-2] * far_mask
    )
    mixed_rows = (gate_b.astype(jnp.float32) * convolved).astype(jnp.bfloat16)
    token_rows = lax.all_to_all(mixed_rows, "tp", split_axis=0, concat_axis=1, tiled=True)
    projected = jnp.dot(token_rows, w_out, preferred_element_type=jnp.float32)
    hidden_state = (resid.astype(jnp.float32) + projected).astype(jnp.bfloat16)
    state_wide = hidden_state.astype(jnp.float32)
    normed = (
        state_wide
        * lax.rsqrt(jnp.mean(state_wide * state_wide, axis=-1, keepdims=True) + 1e-06)
        * norm_gain.astype(jnp.float32)
    ).astype(jnp.bfloat16)
    experts = lax.axis_size("sp") * w_gate.shape[0]
    capacity = 4 * local_rows // experts
    flat_ids = route_ids.reshape(-1)
    one_hot = (flat_ids[:, None] == jnp.arange(experts, dtype=jnp.int32)[None, :]).astype(jnp.int32)
    rank_in = jnp.sum((jnp.cumsum(one_hot, axis=0) - one_hot) * one_hot, axis=1)
    slot_index = flat_ids * capacity + rank_in
    placement = (
        slot_index[:, None] == jnp.arange(experts * capacity, dtype=jnp.int32)[None, :]
    ).astype(jnp.bfloat16)
    repeated = jnp.repeat(normed, 2, axis=0)
    dispatch = jnp.einsum(
        "js,jd->sd", placement, repeated, preferred_element_type=jnp.float32
    ).astype(jnp.bfloat16)
    dispatch = dispatch.reshape(experts, capacity, model_width)
    gathered_piece = lax.all_gather(
        lax.all_to_all(dispatch, "sp", split_axis=0, concat_axis=0, tiled=True),
        "tp",
        axis=0,
        tiled=True,
    )
    flat_rows = gathered_piece.reshape(-1, model_width)
    gate_part = jnp.dot(flat_rows, w_gate[0], preferred_element_type=jnp.float32)
    up_part = jnp.dot(flat_rows, w_up[0], preferred_element_type=jnp.float32)
    activated = (jax.nn.silu(gate_part) * up_part).astype(jnp.bfloat16)
    partial_value = jnp.dot(activated, w_down[0], preferred_element_type=jnp.float32)
    partial_value = partial_value.reshape(
        gathered_piece.shape[0], gathered_piece.shape[1], model_width
    )
    summed = lax.psum_scatter(
        partial_value.astype(jnp.bfloat16), "tp", scatter_dimension=0, tiled=True
    )
    returned = lax.all_to_all(summed, "sp", split_axis=0, concat_axis=0, tiled=True)
    picked = jnp.take(
        returned.reshape(experts * capacity, model_width), slot_index, axis=0
    ).reshape(local_rows, 2, model_width)
    combined = jnp.sum(route_weight[:, :, None] * picked.astype(jnp.float32), axis=1)
    return (hidden_state.astype(jnp.float32) + combined).astype(jnp.bfloat16)


def solution(mesh):
    return jax.shard_map(
        local,
        mesh=mesh,
        in_specs=(
            P("sp", "tp"),
            P("sp", "tp"),
            P("sp", "tp"),
            P(None, "tp"),
            P("sp"),
            P(),
            P(("sp", "tp"), None),
            P(),
            P(("sp", "tp"), None),
            P(("sp", "tp"), None),
            P("sp", None, "tp"),
            P("sp", None, "tp"),
            P("sp", "tp", None),
        ),
        out_specs=P(("sp", "tp"), None),
        check_vma=False,
    )
```

profile of v0, /device:TPU:24, one launch (start us, length us, event | category | flops | bytes accessed | tf_op | source)
XLA Modules:
  0.0 233.2 jit_solution(8225996941570353827)
XLA Ops:
  6.5 0.9 slice.43
  7.4 3.4 %collective-permute-start.1 = (s32[2]{0:T(128)S(1)}, s32[2]{0:T(128)S(1)}, u32[]{:S(2)}, u32[]{:S(2)}) collective-permute-start(s32[2]{0:T(128)S(1)} %slice.43), channel_id=1, source_target_pairs={{0,16},{16,32},{32,48},{48,64},{64,80},{80,96},{96,112},{112,128},... | collective-permute-start | bytes 32 | tf_op jit(solution)/shard_map/ppermute | solution.py:10
  10.8 0.8 slice.38
  11.7 0.8 slice.39
  12.6 3.4 %collective-permute-start = (bf16[2,2,64]{2,1,0:T(2,128)(2,1)S(1)}, bf16[2,2,64]{2,1,0:T(2,128)(2,1)S(1)}, u32[]{:S(2)}, u32[]{:S(2)}) collective-permute-start(bf16[2,2,64]{2,1,0:T(2,128)(2,1)S(1)} %pad_maximum_fusion.1), channel_id=1, source_target_pairs={{0,16},{16,32},{32,48},{48,64},{64,80},{80,96},{96,112},{112,128},... | collective-permute-start | bytes 1544 | tf_op jit(solution)/shard_map/ppermute | solution.py:10
  16.0 0.9 convert_multiply_fusion
  18.3 0.8 copy.51
  19.5 0.8 pad_add_fusion
  21.1 1.0 fusion.19
  22.3 0.8 reshape.97
  23.1 8.6 %all-to-all-start = ((bf16[16,2,1024]{2,1,0:T(2,128)(2,1)}), bf16[16,2,1024]{2,1,0:T(2,128)(2,1)S(1)}, u32[]{:S(2)}, u32[]{:S(2)}) async-start(bf16[16,2,1024]{2,1,0:T(2,128)(2,1)} %reshape.97), calls=%async_computation | async-start | bytes 131072 | tf_op jit(solution)/shard_map/all_to_all | solution.py:50
  31.7 7.7 %all-to-all-done = bf16[16,2,1024]{2,1,0:T(2,128)(2,1)S(1)} async-done(((bf16[16,2,1024]{2,1,0:T(2,128)(2,1)}), bf16[16,2,1024]{2,1,0:T(2,128)(2,1)S(1)}, u32[]{:S(2)}, u32[]{:S(2)}) %all-to-all-start) | async-done | bytes 65568 | tf_op jit(solution)/shard_map/all_to_all | solution.py:50
  39.8 3.1 %multiply_reduce_fusion.1 = (f32[32]{0:T(128)S(1)}, f32[32,2048]{1,0:T(8,128)S(1)}) fusion(bf16[32,1024]{1,0:T(8,128)(2,1)S(1)} %all_to_all.23, bf16[1024,2048]{1,0:T(8,128)(2,1)} %param.18, bf16[32,2048]{1,0:T(8,128)(2,1)} %param.19), kind=kOutput, calls=%fused_computation.20 | convolution fusion | flops 134610912 | bytes 4653184 | tf_op jit(solution)/shard_map/dot_general | solution.py:51
  43.7 16.3 %all_to_all.29 = bf16[16,8,2048]{2,1,0:T(8,128)(2,1)} all-to-all(bf16[16,8,2048]{2,1,0:T(8,128)(2,1)S(1)} %fusion.6), channel_id=1, replica_groups=mesh['sp'=16,'tp'=16] {'sp'}, dimensions={0} | all-to-all | bytes 1048576 | tf_op jit(solution)/shard_map/all_to_all | solution.py:74
  60.1 50.6 %all-gather.2.cloned.1.call-done = bf16[256,8,2048]{2,1,0:T(8,128)(2,1)} async-done(((bf16[16,8,2048]{2,1,0:T(8,128)(2,1)}), bf16[256,8,2048]{2,1,0:T(8,128)(2,1)}) %all-gather.2.cloned.1.call-update) | async-done | bytes 8388624 | tf_op jit(solution)/shard_map/all_gather | solution.py:73
  110.7 7.2 %fusion.2 = f32[2048,448]{0,1:T(8,128)S(1)} fusion(bf16[256,8,2048]{2,1,0:T(8,128)(2,1)} %all-gather.2.cloned.1.call-done, bf16[1,2048,448]{1,2,0:T(8,128)(2,1)} %param.23), kind=kOutput, calls=%fused_computation.3 | convolution fusion | flops 3758096384 | bytes 13893632 | tf_op jit(solution)/shard_map/dot_general | solution.py:80
  117.9 5.5 %multiply_convert_fusion = bf16[2048,448]{0,1:T(8,128)(2,1)} fusion(f32[2048,448]{0,1:T(8,128)S(1)} %fusion.2, bf16[256,8,2048]{2,1,0:T(8,128)(2,1)S(1)} %copy-done.3, bf16[1,2048,448]{1,2,0:T(8,128)(2,1)S(1)} %copy-done.4), kind=kOutput, calls=%fused_computation.6 | convolution fusion | flops 3763601408 | bytes 15728640 | tf_op jit(solution)/shard_map/dot_general | solution.py:81
  123.4 3.8 %copy.54 = bf16[2048,448]{1,0:T(8,128)(2,1)} copy(bf16[2048,448]{0,1:T(8,128)(2,1)} %multiply_convert_fusion) | data formatting | bytes 3670016 | tf_op jit(solution)/shard_map/convert_element_type | solution.py:82
  127.2 9.2 %convolution_convert_fusion = bf16[256,8,2048]{2,0,1:T(8,128)(2,1)} fusion(bf16[256,8,448]{2,1,0:T(8,128)(2,1)} %bitcast.43, bf16[1,448,2048]{2,1,0:T(8,128)(2,1)S(1)} %copy-done), kind=kOutput, calls=%fused_computation.5 | convolution fusion | flops 3762290688 | bytes 12058624 | tf_op jit(solution)/shard_map/dot_general | solution.py:83
  137.4 68.4 %reduce-scatter.2.cloned.1.call-done = bf16[16,8,2048]{2,0,1:T(8,128)(2,1)} async-done(((bf16[256,8,2048]{2,0,1:T(8,128)(2,1)}), bf16[16,8,2048]{2,0,1:T(8,128)(2,1)}) %reduce-scatter.2.cloned.1.call-update) | async-done | bytes 524304 | tf_op jit(solution)/shard_map/reduce_scatter | solution.py:87
  205.8 2.1 copy.56
  208.0 7.2 %all-to-all-start.2 = ((bf16[16,8,2048]{2,1,0:T(8,128)(2,1)}), bf16[16,8,2048]{2,1,0:T(8,128)(2,1)S(1)}, u32[]{:S(2)}, u32[]{:S(2)}) async-start(bf16[16,8,2048]{2,1,0:T(8,128)(2,1)} %copy.56), calls=%async_computation.3 | async-start | bytes 1048576 | tf_op jit(solution)/shard_map/all_to_all | solution.py:90
  215.4 7.6 %all-to-all-done.2 = bf16[16,8,2048]{2,1,0:T(8,128)(2,1)S(1)} async-done(((bf16[16,8,2048]{2,1,0:T(8,128)(2,1)}), bf16[16,8,2048]{2,1,0:T(8,128)(2,1)S(1)}, u32[]{:S(2)}, u32[]{:S(2)}) %all-to-all-start.2) | async-done | bytes 524320 | tf_op jit(solution)/shard_map/all_to_all | solution.py:90
  224.0 1.7 multiply_reduce_fusion
  (52 shorter events, 7.0 us)
Async XLA Ops:
  6.5 120.7 %copy-start = (bf16[1,448,2048]{2,1,0:T(8,128)(2,1)S(1)}, bf16[1,448,2048]{2,1,0:T(8,128)(2,1)}, u32[]{:S(2)}) copy-start(bf16[1,448,2048]{2,1,0:T(8,128)(2,1)} %param.25) | copy-start | bytes 5505028
  7.4 12.1 %collective-permute-start.1 = (s32[2]{0:T(128)S(1)}, s32[2]{0:T(128)S(1)}, u32[]{:S(2)}, u32[]{:S(2)}) collective-permute-start(s32[2]{0:T(128)S(1)} %slice.43), channel_id=1, source_target_pairs={{0,16},{16,32},{32,48},{48,64},{64,80},{80,96},{96,112},{112,128},... | collective-permute-start | bytes 32 | tf_op jit(solution)/shard_map/ppermute | solution.py:10
  12.6 8.4 %collective-permute-start = (bf16[2,2,64]{2,1,0:T(2,128)(2,1)S(1)}, bf16[2,2,64]{2,1,0:T(2,128)(2,1)S(1)}, u32[]{:S(2)}, u32[]{:S(2)}) collective-permute-start(bf16[2,2,64]{2,1,0:T(2,128)(2,1)S(1)} %pad_maximum_fusion.1), channel_id=1, source_target_pairs={{0,16},{16,32},{32,48},{48,64},{64,80},{80,96},{96,112},{112,128},... | collective-permute-start | bytes 1544 | tf_op jit(solution)/shard_map/ppermute | solution.py:10
  23.1 16.4 %all-to-all-start = ((bf16[16,2,1024]{2,1,0:T(2,128)(2,1)}), bf16[16,2,1024]{2,1,0:T(2,128)(2,1)S(1)}, u32[]{:S(2)}, u32[]{:S(2)}) async-start(bf16[16,2,1024]{2,1,0:T(2,128)(2,1)} %reshape.97), calls=%async_computation | async-start | bytes 131072 | tf_op jit(solution)/shard_map/all_to_all | solution.py:50
  31.6 79.1 %all-gather.2.cloned.1.call-start = ((), (), s32[]{:S(2)}) async-start(), calls=%async_computation.4 | async-start | bytes 8912896 | tf_op jit(solution)/shard_map/all_gather | solution.py:73
  60.1 145.8 %reduce-scatter.2.cloned.1.call-start = ((), (), s32[]{:S(2)}) async-start(), calls=%async_computation.5 | async-start | bytes 8912896 | tf_op jit(solution)/shard_map/reduce_scatter | solution.py:87
  110.7 7.2 %copy-start.3 = (bf16[256,8,2048]{2,1,0:T(8,128)(2,1)S(1)}, bf16[256,8,2048]{2,1,0:T(8,128)(2,1)}, u32[]{:S(2)}) copy-start(bf16[256,8,2048]{2,1,0:T(8,128)(2,1)} %all-gather.2.cloned.1.call-done) | copy-start | bytes 25165828
  110.7 7.2 %copy-start.4 = (bf16[1,2048,448]{1,2,0:T(8,128)(2,1)S(1)}, bf16[1,2048,448]{1,2,0:T(8,128)(2,1)}, u32[]{:S(2)}) copy-start(bf16[1,2048,448]{1,2,0:T(8,128)(2,1)} %param.24) | copy-start | bytes 5505028
  136.4 0.7 copy-start.1
  136.4 78.9 %copy-start.2 = (f32[32,2]{0,1:T(2,128)S(1)}, f32[32,2]{0,1:T(2,128)}, u32[]{:S(2)}) copy-start(f32[32,2]{0,1:T(2,128)} %param.22) | copy-start | bytes 772
  208.0 15.1 %all-to-all-start.2 = ((bf16[16,8,2048]{2,1,0:T(8,128)(2,1)}), bf16[16,8,2048]{2,1,0:T(8,128)(2,1)S(1)}, u32[]{:S(2)}, u32[]{:S(2)}) async-start(bf16[16,8,2048]{2,1,0:T(8,128)(2,1)} %copy.56), calls=%async_computation.3 | async-start | bytes 1048576 | tf_op jit(solution)/shard_map/all_to_all | solution.py:90
Sparse Core Ops, SparseCore 0:
  60.2 50.4 all-gather.1
  136.6 69.2 reduce-scatter.1
where the time goes:
time: 235 us; the launch traced here: 233 us
  waiting for transfers between devices  134 us (57%)
  matrix products  25.4 us (11%)
  starting transfers between devices  22.7 us (10%)
  blocking collectives  16.3 us (7%)
  between operations  13.6 us (6%)
  local copies, waits for them, and re-layouts  13.1 us (6%)
  other arithmetic  7.69 us (3%)
    reduce_scatter x1, waiting for transfers between devices, local(): lax.psum_scatter(partial_value.astype(jnp.bfloat16), 'tp', scatter_dimens...  68.4 us
    all_gather x1, waiting for transfers between devices, local(): lax.all_gather(lax.all_to_all(dispatch, 'sp', split_axis=0, concat_axis=0...  50.6 us
    all_to_all x1, blocking collectives, local(): lax.all_to_all(dispatch, 'sp', split_axis=0, concat_axis=0, tiled=True)  16.3 us
    dot_general x1, matrix products, local(): jnp.dot(activated, w_down[0], preferred_element_type=jnp.float32)  9.19 us
    all_to_all x1, starting transfers between devices, local(): lax.all_to_all(mixed_rows, 'tp', split_axis=0, concat_axis=1, tiled=True)  8.57 us
    all_to_all x1, waiting for transfers between devices, local(): lax.all_to_all(mixed_rows, 'tp', split_axis=0, concat_axis=1, tiled=True)  7.73 us
    all_to_all x1, waiting for transfers between devices, local(): lax.all_to_all(summed, 'sp', split_axis=0, concat_axis=0, tiled=True)  7.63 us
    all_to_all x1, starting transfers between devices, local(): lax.all_to_all(summed, 'sp', split_axis=0, concat_axis=0, tiled=True)  7.22 us
  transfers between devices with their start and end apart: 6, of which 4 were waited for; matrix products, arithmetic and copies ran while one was open for 3% of the time, Pallas kernels for 0%

commit v1 on v0

v1 whole, which is shorter than its diff:
```python
import functools

import jax
import jax.numpy as jnp
from jax import lax
from jax.experimental import pallas as pl
from jax.experimental.pallas import tpu as pltpu
from jax.sharding import PartitionSpec as P

MESH = pl.DeviceIdType.MESH
F32 = jnp.float32
BF16 = jnp.bfloat16
NT = (((1,), (1,)), ((), ()))


def kernel(
    S, T, G,
    gb_hbm, gc_hbm, v_hbm, taps_ref, docs_ref, wout_hbm, resid_hbm, gain_ref, ids_ref, rw_ref,
    wg_hbm, wu_hbm, wd_hbm,
    out_ref,
    gb, gc, vin, wout, resid, wg, wu, wd,
    halo_out, halo_in, mix, pieces, dsp, X, Y, YS, YP, R, OUT, RET, hid,
    in_sem, halo_sem, a2a_s, a2a_r, dsp_s, dsp_r, ag_s, ag_r, xd_s, xd_r, yd_s, yd_r,
    rs_s, rs_r, ret_s, ret_r,
):
    sp = lax.axis_index("sp")
    tp = lax.axis_index("tp")
    Z = T // 2
    H = Z // 2
    z = tp // 2
    c = lax.rem(tp, 2)
    mate = tp + 1 - 2 * c
    rows, D = resid.shape
    chl, seq = gb.shape
    cap = dsp.shape[1]
    B = S * cap
    GR = B // G
    SG = S // G
    half = G // 2

    def loc(i, src, dst):
        return pltpu.make_async_copy(src, dst, in_sem.at[i])

    loads = [
        loc(0, gc_hbm, gc), loc(1, v_hbm, vin), loc(2, gb_hbm, gb), loc(3, wout_hbm, wout),
        loc(4, resid_hbm, resid), loc(5, wg_hbm, wg), loc(6, wu_hbm, wu), loc(7, wd_hbm, wd),
    ]
    for copy in loads:
        copy.start()

    barrier = pltpu.get_barrier_semaphore()

    def greet_tp(k, _):
        pl.semaphore_signal(barrier, inc=1, device_id=(sp, lax.rem(tp + k, T)), device_id_type=MESH)
        return 0

    def greet_sp(k, _):
        pl.semaphore_signal(barrier, inc=1, device_id=(lax.rem(sp + k, S), tp), device_id_type=MESH)
        return 0

    lax.fori_loop(1, T, greet_tp, 0)
    lax.fori_loop(1, S, greet_sp, 0)

    def rdma(src, dst, ssem, rsem, dev):
        return pltpu.make_async_remote_copy(
            src_ref=src, dst_ref=dst, send_sem=ssem, recv_sem=rsem, device_id=dev, device_id_type=MESH
        )

    loads[0].wait()
    loads[1].wait()
    product = gc[...].astype(F32) * vin[...].astype(F32)
    docs = docs_ref[...]
    halo_out[0:chl, :] = product[:, seq - 128 :]
    halo_out[chl : chl + 8, :] = jnp.broadcast_to(docs[:, seq - 128 :].astype(F32), (8, 128))

    pl.semaphore_wait(barrier, (T - 1) + (S - 1))

    halo = rdma(halo_out, halo_in, halo_sem.at[0], halo_sem.at[1], (lax.rem(sp + 1, S), tp))
    halo.start()

    lane = lax.broadcasted_iota(jnp.int32, (B, 128), 1)
    slot = lax.broadcasted_iota(jnp.int32, (B, 128), 0)
    ids = jnp.concatenate([ids_ref[...], jnp.full((2, 128 - rows), -1, jnp.int32)], axis=1)
    hit0 = ids[0:1, :] == slot // cap
    hit1 = ids[1:2, :] == slot // cap
    hits = jnp.where(hit0 | hit1, 1.0, 0.0).astype(BF16)
    below = jnp.where(
        lax.broadcasted_iota(jnp.int32, (128, 128), 0) < lax.broadcasted_iota(jnp.int32, (128, 128), 1), 1.0, 0.0
    ).astype(BF16)
    rank = jnp.dot(hits, below, preferred_element_type=F32)
    mine = rank == lax.rem(slot, cap).astype(F32)
    place0 = jnp.where(hit0 & mine, 1.0, 0.0)
    place1 = jnp.where(hit1 & mine, 1.0, 0.0)
    place = (place0 + place1).astype(BF16)

    eye = jnp.where(
        lax.broadcasted_iota(jnp.int32, (chl, chl), 0) == lax.broadcasted_iota(jnp.int32, (chl, chl), 1), 1.0, 0.0
    ).astype(BF16)
    taps = lax.dot_general(eye, taps_ref[...], NT, preferred_element_type=F32)
    loads[2].wait()

    halo.wait()
    before = jnp.concatenate([halo_in[0:chl, :], product], axis=1)
    old_docs = jnp.where(sp > 0, halo_in[chl : chl + 1, :].astype(jnp.int32), -1)
    all_docs = jnp.concatenate([old_docs, docs], axis=1)
    prev1 = pltpu.roll(before, 1, 1)[:, 128:]
    prev2 = pltpu.roll(before, 2, 1)[:, 128:]
    wide_docs = jnp.broadcast_to(all_docs, (8, 128 + seq))
    near = (pltpu.roll(wide_docs, 1, 1)[0:1, 128:] == docs).astype(F32)
    far = (pltpu.roll(wide_docs, 2, 1)[0:1, 128:] == docs).astype(F32)
    conv = taps[:, 2:3] * product + taps[:, 1:2] * prev1 * near + taps[:, 0:1] * prev2 * far
    mixed = (gb[...].astype(F32) * conv).astype(BF16).astype(F32)
    odd = c == 1
    spread = jnp.concatenate([jnp.where(odd, 0.0, mixed), jnp.where(odd, mixed, 0.0)], axis=0)
    mix[...] = spread.T.astype(BF16).reshape(T, rows, 2 * chl)

    def send_piece(k, _):
        p = lax.rem(tp + k, T)
        rdma(mix.at[p], pieces.at[tp], a2a_s.at[p], a2a_r.at[tp], (sp, p)).start()
        return 0

    lax.fori_loop(1, T, send_piece, 0)
    pieces[tp] = mix[tp]

    def take_piece(k, _):
        p = lax.rem(tp + k, T)
        rdma(mix.at[p], pieces.at[p], a2a_s.at[p], a2a_r.at[p], (sp, p)).wait_recv()
        return 0

    loads[3].wait()
    loads[4].wait()
    lax.fori_loop(1, T, take_piece, 0)
    token_rows = jnp.concatenate([pieces[2 * k] + pieces[2 * k + 1] for k in range(Z)], axis=1)
    projected = jnp.dot(token_rows, wout[...], preferred_element_type=F32)
    hidden = (resid[...].astype(F32) + projected).astype(BF16)
    hid[...] = hidden
    wide = hidden.astype(F32)
    normed = (
        wide * lax.rsqrt(jnp.mean(wide * wide, axis=-1, keepdims=True) + 1e-06) * gain_ref[...].astype(F32)
    ).astype(BF16)
    dispatch = jnp.dot(place[:, 0:rows], normed, preferred_element_type=F32).astype(BF16)
    dsp[...] = dispatch.reshape(S, cap, D)

    def slots(ref, s):
        return ref.at[pl.ds(pl.multiple_of(s * cap, cap), cap)]

    def send_rows(k, _):
        e = lax.rem(sp + k, S)
        rdma(dsp.at[e], slots(X.at[tp], sp), dsp_s.at[e], dsp_r.at[sp], (e, tp)).start()
        return 0

    lax.fori_loop(1, S, send_rows, 0)
    own = pltpu.make_async_copy(dsp.at[sp], slots(X.at[tp], sp), dsp_r.at[sp])
    own.start()

    def part(ref, b, g):
        return ref.at[b, pl.ds(pl.multiple_of(g * GR, GR), GR)]

    def up_ok(d, g):
        return (d < H) | ((d == H) & (g < half))

    def down_ok(d, g):
        return (d < H) | ((d == H) & (g >= half))

    above = (sp, 2 * lax.rem(z + 1, Z) + c)
    beneath = (sp, 2 * lax.rem(z + Z - 1, Z) + c)
    other = (sp, mate)

    def ring_gather(way, d, g, b):
        r = part(X, b, g)
        return rdma(r, r, ag_s.at[way, d - 1, g], ag_r.at[way, d - 1, g], above if way == 0 else beneath)

    def share(zz, g):
        r = part(X, 2 * zz + c, g)
        return rdma(r, r, xd_s.at[zz, g], xd_r.at[zz, g], other)

    def take_share(zz, g):
        r = part(X, 2 * zz + 1 - c, g)
        rdma(r, r, xd_s.at[zz, g], xd_r.at[zz, g], other).wait_recv()

    for g in range(G):
        for s in range(g * SG, (g + 1) * SG):
            pltpu.make_async_copy(dsp.at[s], slots(X.at[tp], s), dsp_r.at[s]).wait()
        if 1 < H or g < half:
            ring_gather(0, 1, g, tp).start()
        if 1 < H or g >= half:
            ring_gather(1, 1, g, tp).start()
        share(z, g).start()
    for k in range(5, 8):
        loads[k].wait()

    def expert(d, j):
        @pl.when((d > 0) | (j < 2))
        def _():
            zz = lax.rem(z + Z + jnp.where(j < 2, d, -d), Z)
            core = lax.rem(c + j + jnp.where(d > 0, 1, 0), 2)
            theirs = core != c

            @pl.when(theirs)
            def _():
                for g in range(G):
                    take_share(zz, g)

            x = X[2 * zz + core]
            gate = lax.dot_general(x, wg[...], NT, preferred_element_type=F32)
            up = lax.dot_general(x, wu[...], NT, preferred_element_type=F32)
            act = (gate * jax.nn.sigmoid(gate) * up).astype(BF16)
            y = jnp.dot(act, wd[...], preferred_element_type=F32).astype(BF16)

            @pl.when(theirs)
            def _():
                YS[zz] = y
                rdma(YS.at[zz], YP.at[zz], yd_s.at[zz], yd_r.at[zz], other).start()

            @pl.when(jnp.logical_not(theirs))
            def _():
                Y[zz] = y

    def gather_step(d, g):
        @pl.when(up_ok(d, g))
        def _():
            zz = lax.rem(z + Z - d, Z)
            ring_gather(0, d, g, 2 * zz + c).wait_recv()

            @pl.when(up_ok(d + 1, g))
            def _():
                ring_gather(0, d + 1, g, 2 * zz + c).start()

            share(zz, g).start()

        @pl.when(down_ok(d, g))
        def _():
            zz = lax.rem(z + d, Z)
            ring_gather(1, d, g, 2 * zz + c).wait_recv()

            @pl.when(down_ok(d + 1, g))
            def _():
                ring_gather(1, d + 1, g, 2 * zz + c).start()

            share(zz, g).start()

    def ring_sum(way, d, g, zz):
        return rdma(part(Y, zz, g), part(R.at[way], d - 1, g), rs_s.at[way, d - 1, g], rs_r.at[way, d - 1, g],
                    above if way == 0 else beneath)

    def take_sum(way, d, g, zz):
        rdma(part(Y, zz, g), part(R.at[way], d, g), rs_s.at[way, d, g], rs_r.at[way, d, g],
             above if way == 0 else beneath).wait_recv()

    def take_y(zz):
        rdma(YS.at[zz], YP.at[zz], yd_s.at[zz], yd_r.at[zz], other).wait_recv()

    def rows_of(g):
        return pl.ds(pl.multiple_of(g * GR, GR), GR)

    def sum_start(way, d, g, fresh):
        zz = lax.rem(z + d, Z) if way == 0 else lax.rem(z + Z - d, Z)
        total = Y[zz, rows_of(g)].astype(F32) + YP[zz, rows_of(g)].astype(F32)
        if not fresh:
            take_sum(way, d, g, zz)
            total = total + R[way, d, rows_of(g)].astype(F32)
        Y[zz, rows_of(g)] = total.astype(BF16)
        ring_sum(way, d, g, zz).start()

    def early_sums():
        if H > 1:
            take_y(lax.rem(z + H - 1, Z))
            take_y(lax.rem(z + Z - (H - 1), Z))
            for g in range(half):
                sum_start(0, H - 1, half + g, True)
                sum_start(1, H - 1, g, True)

    steps = H * G

    def step(i, _):
        d = i // G
        j = lax.rem(i, G)

        @pl.when(i == steps)
        def _():
            early_sums()

        @pl.when(j < 4)
        def _():
            expert(d, j)

        if G < 4:
            for extra in range(G, 4):
                @pl.when((j == G - 1) & (i < steps))
                def _():
                    expert(d, extra)

        @pl.when(i < steps)
        def _():
            gather_step(d + 1, j)

        return 0

    lax.fori_loop(0, steps + 2, step, 0)

    take_y(lax.rem(z + H, Z))
    for g in range(half):
        sum_start(0, H, g, True)
        sum_start(1, H, half + g, True)
    if H > 1:
        for g in range(half):
            sum_start(0, H - 1, g, False)
            sum_start(1, H - 1, half + g, False)

    def sum_step(i, _):
        d = H - 2 - i // G
        g = lax.rem(i, G)

        @pl.when(g == 0)
        def _():
            take_y(lax.rem(z + d, Z))
            take_y(lax.rem(z + Z - d, Z))

        sum_start(0, d, g, False)
        sum_start(1, d, g, False)
        return 0

    if H > 2:
        lax.fori_loop(0, (H - 2) * G, sum_step, 0)

    take_y(z)
    for g in range(G):
        lo, hi = g * GR, (g + 1) * GR
        total = Y[z, lo:hi].astype(F32) + YP[z, lo:hi].astype(F32)
        if 1 < H or g < half:
            take_sum(0, 0, g, z)
            total = total + R[0, 0, lo:hi].astype(F32)
        if 1 < H or g >= half:
            take_sum(1, 0, g, z)
            total = total + R[1, 0, lo:hi].astype(F32)
        OUT[g * SG : (g + 1) * SG] = total.astype(BF16).reshape(SG, cap, D)
        for s in range(g * SG, (g + 1) * SG):
            @pl.when(sp != s)
            def _():
                rdma(OUT.at[s], slots(RET, sp), ret_s.at[s], ret_r.at[sp], (s, tp)).start()

            @pl.when(sp == s)
            def _():
                pltpu.make_async_copy(OUT.at[s], slots(RET, s), ret_r.at[s]).start()

    pick0 = place0.T[0:rows].astype(BF16)
    pick1 = place1.T[0:rows].astype(BF16)
    rw = jnp.concatenate([rw_ref[...], jnp.zeros((2, 128 - rows), F32)], axis=1)
    w0 = jnp.broadcast_to(rw[0:1], (128, 128)).T[0:rows, 0:1]
    w1 = jnp.broadcast_to(rw[1:2], (128, 128)).T[0:rows, 0:1]

    for s in range(S):
        pltpu.make_async_copy(OUT.at[s], slots(RET, s), ret_r.at[s]).wait()
    back = RET[...]
    got0 = jnp.dot(pick0, back, preferred_element_type=F32)
    got1 = jnp.dot(pick1, back, preferred_element_type=F32)
    out_ref[...] = (hid[...].astype(F32) + (w0 * got0 + w1 * got1)).astype(BF16)

    halo_done = 0
    del halo_done

    def sent_piece(k, _):
        p = lax.rem(tp + k, T)
        rdma(mix.at[p], pieces.at[p], a2a_s.at[p], a2a_r.at[p], (sp, p)).wait_send()
        return 0

    def sent_rows(k, _):
        e = lax.rem(sp + k, S)
        rdma(dsp.at[e], slots(X.at[tp], e), dsp_s.at[e], dsp_r.at[e], (e, tp)).wait_send()
        rdma(OUT.at[e], slots(RET, e), ret_s.at[e], ret_r.at[e], (e, tp)).wait_send()
        return 0

    lax.fori_loop(1, T, sent_piece, 0)
    lax.fori_loop(1, S, sent_rows, 0)
    for way, ok in ((0, up_ok), (1, down_ok)):
        def sent_ring(i, _):
            d = i // G + 1
            g = lax.rem(i, G)

            @pl.when(ok(d, g))
            def _():
                ring_gather(way, d, g, tp).wait_send()
                ring_sum(way, d, g, z).wait_send()

            return 0

        lax.fori_loop(0, steps, sent_ring, 0)

    def sent_share(i, _):
        share(i // G, lax.rem(i, G)).wait_send()
        return 0

    def sent_y(zz, _):
        rdma(YS.at[zz], YP.at[zz], yd_s.at[zz], yd_r.at[zz], other).wait_send()
        return 0

    lax.fori_loop(0, Z * G, sent_share, 0)
    lax.fori_loop(0, Z, sent_y, 0)


def local(
    gate_b, gate_c, values_in, conv_w, documents, w_out, resid, norm_gain, route_ids, route_weight,
    w_gate, w_up, w_down,
):
    S, T = lax.axis_size("sp"), lax.axis_size("tp")
    seq, chl = gate_b.shape
    rows, D = resid.shape
    cap = 4 * rows // S
    fh = w_gate.shape[2]
    B = S * cap
    G = 4 if S % 4 == 0 else 2
    Z = T // 2
    H = Z // 2
    vm = pl.BlockSpec(memory_space=pltpu.VMEM)
    hbm = pl.BlockSpec(memory_space=pl.ANY)
    dma = pltpu.SemaphoreType.DMA
    scratch = [
        pltpu.VMEM((chl, seq), BF16), pltpu.VMEM((chl, seq), BF16), pltpu.VMEM((chl, seq), BF16),
        pltpu.VMEM(w_out.shape, BF16), pltpu.VMEM((rows, D), BF16),
        pltpu.VMEM((fh, D), BF16), pltpu.VMEM((fh, D), BF16), pltpu.VMEM((fh, D), BF16),
        pltpu.VMEM((chl + 8, 128), F32), pltpu.VMEM((chl + 8, 128), F32),
        pltpu.VMEM((T, rows, 2 * chl), BF16), pltpu.VMEM((T, rows, 2 * chl), BF16),
        pltpu.VMEM((S, cap, D), BF16),
        pltpu.VMEM((T, B, D), BF16),
        pltpu.VMEM((Z, B, D), BF16), pltpu.VMEM((Z, B, D), BF16), pltpu.VMEM((Z, B, D), BF16),
        pltpu.VMEM((2, H, B, D), BF16),
        pltpu.VMEM((S, cap, D), BF16), pltpu.VMEM((B, D), BF16), pltpu.VMEM((rows, D), BF16),
        dma((8,)), dma((2,)), dma((T,)), dma((T,)), dma((S,)), dma((S,)),
        dma((2, H, G)), dma((2, H, G)), dma((Z, G)), dma((Z, G)), dma((Z,)), dma((Z,)),
        dma((2, H, G)), dma((2, H, G)), dma((S,)), dma((S,)),
    ]
    return pl.pallas_call(
        functools.partial(kernel, S, T, G),
        out_shape=jax.ShapeDtypeStruct((rows, D), BF16),
        in_specs=[hbm, hbm, hbm, vm, vm, hbm, hbm, vm, vm, vm, hbm, hbm, hbm],
        out_specs=vm,
        scratch_shapes=scratch,
        compiler_params=pltpu.CompilerParams(
            collective_id=0, has_side_effects=True, vmem_limit_bytes=60 * 1024 * 1024
        ),
    )(
        gate_b.T, gate_c.T, values_in.T, conv_w, documents.reshape(1, seq), w_out, resid,
        norm_gain.reshape(1, D), route_ids.T, route_weight.T,
        jnp.swapaxes(w_gate, 1, 2)[0], jnp.swapaxes(w_up, 1, 2)[0], w_down[0],
    )


def solution(mesh):
    return jax.shard_map(
        local,
        mesh=mesh,
        in_specs=(
            P("sp", "tp"), P("sp", "tp"), P("sp", "tp"), P(None, "tp"), P("sp"), P(),
            P(("sp", "tp"), None), P(), P(("sp", "tp"), None), P(("sp", "tp"), None),
            P("sp", None, "tp"), P("sp", None, "tp"), P("sp", "tp", None),
        ),
        out_specs=P(("sp", "tp"), None),
        check_vma=False,
    )
```

time: 235 us -> 130 us (0.55)
  waiting for transfers between devices: 134 us -> 0 us
  Pallas kernels: 0 us -> 127 us
  matrix products: 25.4 us -> 0 us
  starting transfers between devices: 22.7 us -> 0 us
  blocking collectives: 16.3 us -> 0 us
  between operations: 13.6 us -> 0.01 us
  local copies, waits for them, and re-layouts: 13.1 us -> 2.86 us
  other arithmetic: 7.69 us -> 0 us
    pallas_call x0 -> x1, Pallas kernels: none -> 127 us  [local(): pl.pallas_call(functools.partial(kernel, S, T, G), out_shape=jax.ShapeDty...]
    reduce_scatter x1 -> x0, waiting for transfers between devices: 68.4 us -> none  [local(): lax.psum_scatter(partial_value.astype(jnp.bfloat16), 'tp', scatter_dimens...]
    all_gather x1 -> x0, waiting for transfers between devices: 50.6 us -> none  [local(): lax.all_gather(lax.all_to_all(dispatch, 'sp', split_axis=0, concat_axis=0...]
    dot_general x5 -> x0, matrix products: 25.4 us -> none  [the longest x1 9.19 us: local(): jnp.dot(activated, w_down[0], preferred_element_type=jnp.float32)]
    all_to_all x1 -> x0, blocking collectives: 16.3 us -> none  [local(): lax.all_to_all(dispatch, 'sp', split_axis=0, concat_axis=0, tiled=True)]
    all_to_all x2 -> x0, starting transfers between devices: 15.8 us -> none  [the longest x1 8.57 us: local(): lax.all_to_all(mixed_rows, 'tp', split_axis=0, concat_axis=1, tiled=True)]
    all_to_all x2 -> x0, waiting for transfers between devices: 15.4 us -> none  [the longest x1 7.73 us: local(): lax.all_to_all(mixed_rows, 'tp', split_axis=0, concat_axis=1, tiled=True)]
    ppermute x2 -> x0, starting transfers between devices: 6.79 us -> none  [passed_along(): return lax.ppermute(block, axis, route)]
  transfers between devices with their start and end apart: 6 -> 0, of which waited for: 4 -> 0; matrix products, arithmetic and copies ran while one was open for 3% -> 0% of each run, Pallas kernels for 0% -> 0%
where the time goes in v1:
time: 130 us
  Pallas kernels  127 us (98%)
  local copies, waits for them, and re-layouts  2.86 us (2%)
    pallas_call x1, Pallas kernels, local(): pl.pallas_call(functools.partial(kernel, S, T, G), out_shape=jax.ShapeDty...  127 us

profile of v1, /device:TPU:24, one launch (start us, length us, event | category | flops | bytes accessed | tf_op | source)
XLA Modules:
  0.0 129.8 jit_solution(14169429538030291830)
XLA Ops:
  0.0 1.3 reshape.7.gain_ref
  1.3 126.9 %shard_map.127 = bf16[32,2048]{1,0:T(8,128)(2,1)} custom-call(bf16[64,512]{1,0:T(8,128)(2,1)} %bitcast.16, bf16[64,512]{1,0:T(8,128)(2,1)} %bitcast.17, bf16[64,512]{1,0:T(8,128)(2,1)} %bitcast.18, bf16[3,64]{1,0:T(4,128)(2,1)} %taps_ref.1, s32[1,512]{1,0:T(1,128)} %bitcast.19, bf16[1024,2048]{1,0:T(8,128)(2,1)} %wout_hbm.1, bf16[32,2048]{1,0:T(8,128)(2,1)} %resid_hbm.1, ...), custom_call_target="tpu_custom_call" | custom-call | tf_op jit(solution)/shard_map/pallas_call | solution.py:432
  128.2 1.6 %copy.15 = bf16[32,2048]{1,0:T(8,128)(2,1)} copy(bf16[32,2048]{1,0:T(8,128)(2,1)} %shard_map.127) | data formatting | bytes 262144
